TPU v7x, 32 devices: a whole 2x2x4 slice. The times are simulated.
32 devices in a mesh: grp: 2 (over y), fs: 4 (over z), tp: 4 (over x, core).
Axes of the slice: x: 2, y: 2, z: 4, core: 2. Of those that a mesh axis runs over, the one named last changes fastest.
Arguments:
- incoming_representations: bfloat16 [5120, 2048], P(('grp', 'fs', 'tp')), parts along dimension 0, may hold values from -6 to 6
- perceptron_switch_coefficients: bfloat16 [2048, 5120], P('fs', 'tp'), may hold values from -0.125 to 0.125
- perceptron_expand_coefficients: bfloat16 [2048, 5120], P('fs', 'tp'), may hold values from -0.125 to 0.125
- perceptron_contract_coefficients: bfloat16 [5120, 2048], P('tp', 'fs'), may hold values from -0.5 to 0.5
- probe_coefficients: bfloat16 [2048, 512], P('fs', 'tp'), may hold values from -0.125 to 0.125
- address_coefficients: bfloat16 [2048, 512], P('fs', 'tp'), may hold values from -0.125 to 0.125
- payload_coefficients: bfloat16 [2048, 1024], P('fs', 'tp'), may hold values from -0.125 to 0.125
- emit_switch_coefficients: bfloat16 [2048, 1024], P('fs', 'tp'), may hold values from -0.125 to 0.125
- forgetting_shrink_coefficients: bfloat16 [2048, 32], replicated, may hold values from -0.125 to 0.125
- forgetting_expand_coefficients: bfloat16 [32, 512], P(None, 'tp'), may hold values from -3 to 3
- forgetting_sigmoid_intercept: float32 [512], P('tp'), may hold values from -1 to 9
- extra_forgetting_logits: float32 [5120, 512], P(('grp', 'fs'), 'tp'), parts along dimension 0, may hold values from -0.7 to 0
- subspace_rescaling_amplitude: float32 [128], replicated, may hold values from 0.1 to 1.9
- recurrence_emit_coefficients: bfloat16 [1024, 2048], P('tp', 'fs'), may hold values from -0.5 to 0.5
Outputs:
- layer_out: bfloat16 [5120, 2048], P(('grp', 'fs', 'tp')), parts along dimension 0
There are 2 independent parts, one for each index of `grp`. A program takes and returns all parts, laid end to end along the dimension named above; an argument that names none is the same for every part. Nothing has to cross between parts.
All inputs are finite; a program needn't handle non-finite values.
Results may differ from a plain program's by a relative error of at most 0.035.
Values may be sent and summed in bfloat16 or wider, within the bound.
A program may use at most 64 MiB of HBM per device.

v0:
```python
import jax
import jax.numpy as jnp
from jax import lax
from jax.sharding import PartitionSpec as P

DK = 64
DV = 128
BLOCK = 64
SEQUENCE_LENGTH = 320


residual_gain = 1.681792830507429
forgetting_steepness_multiplier = 16.0
epsilon = 1e-06
highest = lax.Precision.HIGHEST


def post_norm(residual, branch):
    summed = residual_gain * residual.astype(jnp.float32) + branch
    average = jnp.mean(summed, axis=-1, keepdims=True)
    centred = summed - average
    variance = jnp.mean(centred * centred, axis=-1, keepdims=True)
    return (centred * lax.rsqrt(variance + epsilon)).astype(jnp.bfloat16)


def gather_group(stored):
    return lax.all_gather(stored, "tp", axis=0, tiled=True)


def return_rows(hidden, weight_full):
    return lax.psum_scatter(
        jnp.dot(hidden, weight_full, preferred_element_type=jnp.float32).astype(jnp.bfloat16),
        "tp",
        scatter_dimension=0,
        tiled=True,
    ).astype(jnp.float32)


def blockwise_mixing(queries, key_rows, values, forgetting_euler_power):
    token_count = queries.shape[0]
    head_count = queries.shape[1] // DK
    seq_count = token_count // SEQUENCE_LENGTH
    block_count = SEQUENCE_LENGTH // BLOCK

    def to_blocks(source, channels):
        shaped = source.astype(jnp.float32).reshape(
            seq_count, block_count, BLOCK, head_count, channels
        )
        return shaped.transpose(0, 3, 1, 2, 4)

    query_blk = to_blocks(queries, DK)
    key_blk = to_blocks(key_rows, DK)
    value_blk = to_blocks(values, DV)
    decay_blk = to_blocks(forgetting_euler_power, DK)
    inclusive = jnp.cumsum(decay_blk, axis=3)
    exclusive = inclusive - decay_blk
    block_end = inclusive[:, :, :, BLOCK - 1 :, :]
    token_positions = jnp.arange(BLOCK)
    lower_mask = (token_positions[:, None] >= token_positions[None, :])[:, :, None]
    flat_lead = seq_count * head_count * block_count

    def flatten(source):
        return source.reshape((flat_lead, BLOCK, source.shape[-1]))

    def within_block(inputs):
        query_one, key_one, value_one, incl_one, excl_one = inputs
        spread = jnp.where(
            lower_mask,
            incl_one[:, None, :] - incl_one[None, :, :],
            excl_one[None, :, :] - excl_one[:, None, :],
        )
        scores = jnp.sum(query_one[:, None, :] * key_one[None, :, :] * jnp.exp(spread), axis=-1)
        return jnp.dot(scores, value_one, precision=highest)

    local_out = lax.map(
        within_block,
        (
            flatten(query_blk),
            flatten(key_blk),
            flatten(value_blk),
            flatten(inclusive),
            flatten(exclusive),
        ),
    )
    local_out = local_out.reshape(value_blk.shape)
    forward_keys = key_blk * jnp.exp(block_end - inclusive)
    backward_keys = key_blk * jnp.exp(exclusive)
    forward_sums = jnp.einsum("shnld,shnlv->nshdv", forward_keys, value_blk, precision=highest)
    backward_sums = jnp.einsum("shnld,shnlv->nshdv", backward_keys, value_blk, precision=highest)
    through = jnp.moveaxis(jnp.exp(block_end[:, :, :, 0, :]), 2, 0)

    def advance(carried, inputs):
        block_sum, segment_passing_across = inputs
        return (segment_passing_across[..., None] * carried + block_sum, carried)

    start_state = jnp.zeros(forward_sums.shape[1:], jnp.float32)
    _, before = lax.scan(advance, start_state, (forward_sums, through))
    _, after = lax.scan(advance, start_state, (backward_sums, through), reverse=True)
    carried_out = jnp.einsum(
        "shnld,nshdv->shnlv", query_blk * jnp.exp(inclusive), before, precision=highest
    )
    carried_out = carried_out + jnp.einsum(
        "shnld,nshdv->shnlv", query_blk * jnp.exp(block_end - exclusive), after, precision=highest
    )
    combined = local_out + carried_out
    return combined.transpose(0, 2, 3, 1, 4).reshape(token_count, head_count, DV)


def per_device(
    incoming_representations,
    perceptron_switch_coefficients,
    perceptron_expand_coefficients,
    perceptron_contract_coefficients,
    probe_coefficients,
    address_coefficients,
    payload_coefficients,
    emit_switch_coefficients,
    forgetting_shrink_coefficients,
    forgetting_expand_coefficients,
    forgetting_sigmoid_intercept,
    extra_forgetting_logits,
    subspace_rescaling_amplitude,
    recurrence_emit_coefficients,
):

    def expand(gathered):
        return (
            jnp.dot(
                gathered,
                lax.all_gather(perceptron_switch_coefficients, "fs", axis=0, tiled=True),
                preferred_element_type=jnp.float32,
            ),
            jnp.dot(
                gathered,
                lax.all_gather(perceptron_expand_coefficients, "fs", axis=0, tiled=True),
                preferred_element_type=jnp.float32,
            ),
        )

    def channel_half(stored):
        gathered = gather_group(stored)
        gate_sum, up_sum = expand(gathered)
        hidden = (jax.nn.silu(gate_sum) * up_sum).astype(jnp.bfloat16)
        return post_norm(
            stored,
            0.5
            * return_rows(
                hidden, lax.all_gather(perceptron_contract_coefficients, "fs", axis=1, tiled=True)
            ),
        )

    opening_perceptron_result = channel_half(incoming_representations)
    gathered = gather_group(opening_perceptron_result)
    pieces = (
        lax.all_gather(probe_coefficients, "fs", axis=0, tiled=True),
        lax.all_gather(address_coefficients, "fs", axis=0, tiled=True),
        lax.all_gather(payload_coefficients, "fs", axis=0, tiled=True),
        lax.all_gather(emit_switch_coefficients, "fs", axis=0, tiled=True),
    )
    projected = tuple(
        (jnp.dot(gathered, piece_one, preferred_element_type=jnp.float32) for piece_one in pieces)
    )
    queries, key_rows, values, outgate = [summed.astype(jnp.bfloat16) for summed in projected]
    compact_inner_dimensionality = jnp.dot(
        gathered, forgetting_shrink_coefficients, preferred_element_type=jnp.float32
    ).astype(jnp.bfloat16)
    forgetting_euler_power = (
        jax.nn.log_sigmoid(
            jnp.dot(
                compact_inner_dimensionality,
                forgetting_expand_coefficients,
                preferred_element_type=jnp.float32,
            )
            + forgetting_sigmoid_intercept
        )
        / forgetting_steepness_multiplier
        + extra_forgetting_logits
    )
    mixed_heads = blockwise_mixing(queries, key_rows, values, forgetting_euler_power)
    scaled = (
        mixed_heads
        * lax.rsqrt(jnp.mean(mixed_heads * mixed_heads, axis=-1, keepdims=True) + epsilon)
        * subspace_rescaling_amplitude
    )
    opener = jax.nn.silu(outgate.astype(jnp.float32)).reshape(mixed_heads.shape)
    gated = (scaled * opener).reshape(mixed_heads.shape[0], -1).astype(jnp.bfloat16)
    out_full = lax.all_gather(recurrence_emit_coefficients, "fs", axis=1, tiled=True)
    context_blend_result = post_norm(opening_perceptron_result, return_rows(gated, out_full))
    return channel_half(context_blend_result)


def solution(mesh):
    return jax.shard_map(
        per_device,
        mesh=mesh,
        in_specs=(
            P(("grp", "fs", "tp"), None),
            P("fs", "tp"),
            P("fs", "tp"),
            P("tp", "fs"),
            P("fs", "tp"),
            P("fs", "tp"),
            P("fs", "tp"),
            P("fs", "tp"),
            P(),
            P(None, "tp"),
            P("tp"),
            P(("grp", "fs"), "tp"),
            P(),
            P("tp", "fs"),
        ),
        out_specs=P(("grp", "fs", "tp"), None),
        check_vma=False,
    )
```

profile of v0, /device:TPU:0, one launch (start us, length us, event | category | flops | bytes accessed | tf_op | source)
XLA Modules:
  0.0 716.5 jit_solution(12505510455766262346)
XLA Ops:
  9.4 27.8 %all-gather.10.cloned.1.call-done = bf16[640,2048]{1,0:T(8,128)(2,1)} async-done(((bf16[160,2048]{1,0:T(8,128)(2,1)}), bf16[640,2048]{1,0:T(8,128)(2,1)}) %all-gather.10.cloned.1.call-update) | async-done | bytes 2621456 | tf_op jit(solution)/shard_map/all_gather | solution.py:27
  37.2 99.6 %all-gather.12.cloned.1.call-done = bf16[2048,1280]{1,0:T(8,128)(2,1)} async-done(((bf16[512,1280]{1,0:T(8,128)(2,1)}), bf16[2048,1280]{1,0:T(8,128)(2,1)}) %all-gather.12.cloned.1.call-update) | async-done | bytes 5242896 | tf_op jit(solution)/shard_map/all_gather | solution.py:130
  136.8 8.5 %fusion.46 = f32[640,1280]{1,0:T(8,128)} fusion(bf16[640,2048]{1,0:T(8,128)(2,1)} %all-gather.10.cloned.1.call-done, bf16[2048,1280]{1,0:T(8,128)(2,1)} %all-gather.12.cloned.1.call-done), kind=kOutput, calls=%fused_computation.97 | convolution fusion | flops 3355443200 | bytes 11141120 | tf_op jit(solution)/shard_map/dot_general | solution.py:128
  145.4 89.4 %all-gather.14.cloned.1.call-done = bf16[2048,1280]{1,0:T(8,128)(2,1)} async-done(((bf16[512,1280]{1,0:T(8,128)(2,1)}), bf16[2048,1280]{1,0:T(8,128)(2,1)}) %all-gather.14.cloned.1.call-update) | async-done | bytes 5242896 | tf_op jit(solution)/shard_map/all_gather | solution.py:135
  234.8 97.8 %all-gather.16.cloned.1.call-done = bf16[1280,2048]{1,0:T(8,128)(2,1)} async-done(((bf16[1280,512]{1,0:T(8,128)(2,1)}), bf16[1280,2048]{1,0:T(8,128)(2,1)}) %all-gather.16.cloned.1.call-update) | async-done | bytes 5242896 | tf_op jit(solution)/shard_map/all_gather | solution.py:148
  332.6 14.4 %convolution_convert_fusion.2 = bf16[640,2048]{1,0:T(8,128)(2,1)} fusion(bf16[1280,2048]{1,0:T(8,128)(2,1)} %all-gather.16.cloned.1.call-done, bf16[640,2048]{1,0:T(8,128)(2,1)S(1)} %copy-done.18, bf16[2048,1280]{1,0:T(8,128)(2,1)} %all-gather.14.cloned.1.call-done, f32[640,1280]{1,0:T(8,128)} %fusion.46), kind=kOutput, calls=%fused_computation.23 | convolution fusion | flops 6717112320 | bytes 19005440 | tf_op jit(solution)/shard_map/dot_general | solution.py:32
  347.1 32.9 %reduce-scatter.4.cloned.1.call-done = bf16[160,2048]{1,0:T(8,128)(2,1)} async-done(((bf16[640,2048]{1,0:T(8,128)(2,1)}), bf16[160,2048]{1,0:T(8,128)(2,1)}) %reduce-scatter.4.cloned.1.call-update) | async-done | bytes 655376 | tf_op jit(solution)/shard_map/reduce_scatter | solution.py:31
  386.7 16.0 %all_gather.42 = bf16[2048,128]{1,0:T(8,128)(2,1)} all-gather(bf16[512,128]{1,0:T(8,128)(2,1)S(1)} %copy-done.13), channel_id=1, replica_groups=mesh['grp'=2,'fs'=4,'tp'=4] {'fs'}, dimensions={0}, use_global_device_ids=true | all-gather | bytes 655360 | tf_op jit(solution)/shard_map/all_gather | solution.py:156
  402.7 17.1 %all_gather.41 = bf16[2048,128]{1,0:T(8,128)(2,1)} all-gather(bf16[512,128]{1,0:T(8,128)(2,1)S(1)} %copy-done.14), channel_id=1, replica_groups=mesh['grp'=2,'fs'=4,'tp'=4] {'fs'}, dimensions={0}, use_global_device_ids=true | all-gather | bytes 655360 | tf_op jit(solution)/shard_map/all_gather | solution.py:155
  420.4 2.9 fusion.31
  424.6 2.0 copy.138
  426.6 2.5 reduce_window_sum.11
  430.0 1.9 fusion.13
  433.1 2.0 copy.65
  435.2 3.0 bitcast_multiply_fusion.2
  439.7 2.8 convolution_convert_fusion.4
  444.5 2.6 fusion.21
  448.0 8.6 %while.43 = (s32[]{:T(128)}, f32[2,2,64,128]{3,2,1,0:T(8,128)S(1)}, f32[5,2,2,64,128]{4,3,0,2,1:T(8,128)}, f32[5,2,2,64]{3,2,1,0:T(2,128)S(1)}, f32[5,2,2,64,128...) while((s32[]{:T(128)}, f32[2,2,64,128]{3,2,1,0:T(8,128)S(1)}, ...), condition=%wide.region_10.11_spmd.clone, body=%wide.region_9.10_spmd.clone.sunk | while | flops 131076 | bytes 658552 | solution.py:98
  456.6 2.6 fusion.23
  459.2 2.6 fusion.14
  464.1 2.0 copy.68
  466.1 90.3 %while.41 = (s32[]{:T(128)}, f32[20,64,128]{2,1,0:T(8,128)}, f32[20,64,64]{2,1,0:T(8,128)}, f32[20,64,64]{2,1,0:T(8,128)}, f32[20,64,64]{2,1,0:T(8,128)}, /*inde...) while((s32[]{:T(128)}, f32[20,64,128]{2,1,0:T(8,128)}, f32[20,64,64]{2,1,0:T(8,128)}, ...), condition=%wide.region_6.7_spmd.clone, body=%wide.region_4.6_spmd.clone.sunk | while | flops 7864322 | bytes 304221 | solution.py:75
  557.3 11.9 %while.42 = (s32[]{:T(128)}, f32[2,2,64,128]{3,2,1,0:T(8,128)S(1)}, f32[5,2,2,64,128]{4,3,0,2,1:T(8,128)}, f32[5,2,2,64]{3,2,1,0:T(2,128)}, f32[5,2,2,64,128]{4,3,2,1,0:T(8,128)}, /*index=5*/s32[]{:T(128)}, s32[]{:T(128)}) while((s32[]{:T(128)}, f32[2,2,64,128]{3,2,1,0:T(8,128)S(1)}, f32[5,2,2,64,128]{4,3,0,2,1:T(8,128)}, ...), condition=%wide.region_8.9_spmd.clone, body=%wide.region_7.8_spmd.clone.sunk | while | flops 131075 | bytes 659040 | solution.py:97
  569.2 2.3 fusion.25
  571.5 1.8 multiply_reduce_fusion.4
  573.5 2.4 copy.77
  577.5 6.3 convolution_convert_fusion.1
  583.8 34.0 %reduce-scatter.6.cloned.1.call-done = bf16[160,2048]{1,0:T(8,128)(2,1)} async-done(((bf16[640,2048]{1,0:T(8,128)(2,1)}), bf16[160,2048]{1,0:T(8,128)(2,1)}) %reduce-scatter.6.cloned.1.call-update) | async-done | bytes 655376 | tf_op jit(solution)/shard_map/reduce_scatter | solution.py:31
  622.2 25.4 %all-gather.26.cloned.1.call-done = bf16[640,2048]{1,0:T(8,128)(2,1)} async-done(((bf16[160,2048]{1,0:T(8,128)(2,1)}), bf16[640,2048]{1,0:T(8,128)(2,1)}) %all-gather.26.cloned.1.call-update) | async-done | bytes 2621456 | tf_op jit(solution)/shard_map/all_gather | solution.py:27
  647.6 8.7 %fusion.47 = f32[640,1280]{1,0:T(8,128)} fusion(bf16[640,2048]{1,0:T(8,128)(2,1)} %all-gather.26.cloned.1.call-done, bf16[2048,1280]{1,0:T(8,128)(2,1)} %all-gather.12.cloned.1.call-done), kind=kOutput, calls=%fused_computation.98 | convolution fusion | flops 3355443200 | bytes 11141120 | tf_op jit(solution)/shard_map/dot_general | solution.py:128
  656.3 14.5 %convolution_convert_fusion = bf16[640,2048]{1,0:T(8,128)(2,1)} fusion(bf16[1280,2048]{1,0:T(8,128)(2,1)} %all-gather.16.cloned.1.call-done, bf16[640,2048]{1,0:T(8,128)(2,1)S(1)} %copy-done.19, bf16[2048,1280]{1,0:T(8,128)(2,1)} %all-gather.14.cloned.1.call-done, f32[640,1280]{1,0:T(8,128)} %fusion.47), kind=kOutput, calls=%fused_computation.21 | convolution fusion | flops 6717112320 | bytes 19005440 | tf_op jit(solution)/shard_map/dot_general | solution.py:32
  670.8 34.6 %reduce-scatter.8.cloned.1.call-done = bf16[160,2048]{1,0:T(8,128)(2,1)} async-done(((bf16[640,2048]{1,0:T(8,128)(2,1)}), bf16[160,2048]{1,0:T(8,128)(2,1)}) %reduce-scatter.8.cloned.1.call-update) | async-done | bytes 655376 | tf_op jit(solution)/shard_map/reduce_scatter | solution.py:31
  (237 shorter events, 141.6 us)
Async XLA Ops:
  6.5 413.9 %copy-start = (bf16[2048,32]{0,1:T(8,128)(2,1)S(1)}, bf16[2048,32]{0,1:T(8,128)(2,1)}, u32[]{:S(2)}) copy-start(bf16[2048,32]{0,1:T(8,128)(2,1)} %param.28) | copy-start | bytes 393220
  6.5 30.6 %all-gather.10.cloned.1.call-start = ((), (), s32[]{:S(2)}) async-start(), calls=%async_computation.3 | async-start | bytes 3276800 | tf_op jit(solution)/shard_map/all_gather | solution.py:27
  7.3 129.6 %all-gather.12.cloned.1.call-start = ((), (), s32[]{:S(2)}) async-start(), calls=%async_computation.4 | async-start | bytes 6553600 | tf_op jit(solution)/shard_map/all_gather | solution.py:130
  8.0 226.8 %all-gather.14.cloned.1.call-start = ((), (), s32[]{:S(2)}) async-start(), calls=%async_computation.5 | async-start | bytes 6553600 | tf_op jit(solution)/shard_map/all_gather | solution.py:135
  8.7 323.9 %all-gather.16.cloned.1.call-start = ((), (), s32[]{:S(2)}) async-start(), calls=%async_computation.6 | async-start | bytes 6553600 | tf_op jit(solution)/shard_map/all_gather | solution.py:148
  9.3 370.7 %reduce-scatter.4.cloned.1.call-start = ((), (), s32[]{:S(2)}) async-start(), calls=%async_computation.7 | async-start | bytes 3276800 | tf_op jit(solution)/shard_map/reduce_scatter | solution.py:31
  37.2 295.4 %copy-start.18 = (bf16[640,2048]{1,0:T(8,128)(2,1)S(1)}, bf16[640,2048]{1,0:T(8,128)(2,1)}, u32[]{:S(2)}) copy-start(bf16[640,2048]{1,0:T(8,128)(2,1)} %all-gather.10.cloned.1.call-done) | copy-start | bytes 7864324
  347.0 33.0 %copy-start.5 = (bf16[160,2048]{1,0:T(8,128)(2,1)S(1)}, bf16[160,2048]{1,0:T(8,128)(2,1)}, u32[]{:S(2)}) copy-start(bf16[160,2048]{1,0:T(8,128)(2,1)} %param.20) | copy-start | bytes 1966084
  347.0 73.4 %all-gather.18.cloned.1.call-start = ((), (), s32[]{:S(2)}) async-start(), calls=%async_computation.8 | async-start | bytes 3276800 | tf_op jit(solution)/shard_map/all_gather | solution.py:27
  380.0 3.1 copy-start.7
  381.5 5.2 copy-start.13
  383.1 19.6 %copy-start.14 = (bf16[512,128]{1,0:T(8,128)(2,1)S(1)}, bf16[512,128]{1,0:T(8,128)(2,1)}, u32[]{:S(2)}) copy-start(bf16[512,128]{1,0:T(8,128)(2,1)} %param.24) | copy-start | bytes 393220
  383.1 36.7 %copy-start.20 = (f32[128]{0:T(128)S(1)}, f32[128]{0:T(128)}, u32[]{:S(2)}) copy-start(f32[128]{0:T(128)} %param.32) | copy-start | bytes 1540
  383.1 37.3 %copy-start.12 = (f32[640,128]{1,0:T(8,128)S(1)}, f32[640,128]{1,0:T(8,128)}, u32[]{:S(2)}) copy-start(f32[640,128]{1,0:T(8,128)} %param.31) | copy-start | bytes 983044
  383.1 37.3 %copy-start.16 = (bf16[32,128]{1,0:T(8,128)(2,1)S(1)}, bf16[32,128]{1,0:T(8,128)(2,1)}, u32[]{:S(2)}) copy-start(bf16[32,128]{1,0:T(8,128)(2,1)} %param.29) | copy-start | bytes 24580
  383.2 37.2 %copy-start.17 = (f32[128]{0:T(128)S(1)}, f32[128]{0:T(128)}, u32[]{:S(2)}) copy-start(f32[128]{0:T(128)} %param.30) | copy-start | bytes 1540
  384.4 55.3 %all-gather.20.cloned.1.call-start = ((), (), s32[]{:S(2)}) async-start(), calls=%async_computation.9 | async-start | bytes 1310720 | tf_op jit(solution)/shard_map/all_gather | solution.py:157
  385.1 190.8 %all-gather.22.cloned.1.call-start = ((), (), s32[]{:S(2)}) async-start(), calls=%async_computation.10 | async-start | bytes 1310720 | tf_op jit(solution)/shard_map/all_gather | solution.py:158
  385.9 190.1 %all-gather.24.cloned.1.call-start = ((), (), s32[]{:S(2)}) async-start(), calls=%async_computation.11 | async-start | bytes 1310720 | tf_op jit(solution)/shard_map/all_gather | solution.py:187
  386.6 231.2 %reduce-scatter.6.cloned.1.call-start = ((), (), s32[]{:S(2)}) async-start(), calls=%async_computation.12 | async-start | bytes 3276800 | tf_op jit(solution)/shard_map/reduce_scatter | solution.py:31
  423.3 6.7 copy-start.2
  456.6 5.3 copy-start.15
  569.2 2.3 copy-start.9
  573.3 4.2 copy-start.21
  583.8 34.1 %copy-start.3 = (bf16[160,2048]{1,0:T(8,128)(2,1)S(1)}, bf16[160,2048]{1,0:T(8,128)(2,1)}, u32[]{:S(2)}) copy-start(bf16[160,2048]{1,0:T(8,128)(2,1)} %multiply_convert_fusion.2) | copy-start | bytes 1966084
  583.8 63.9 %all-gather.26.cloned.1.call-start = ((), (), s32[]{:S(2)}) async-start(), calls=%async_computation.13 | async-start | bytes 3276800 | tf_op jit(solution)/shard_map/all_gather | solution.py:27
  617.9 2.9 copy-start.6
  622.0 83.5 %reduce-scatter.8.cloned.1.call-start = ((), (), s32[]{:S(2)}) async-start(), calls=%async_computation.14 | async-start | bytes 3276800 | tf_op jit(solution)/shard_map/reduce_scatter | solution.py:31
  647.6 8.7 %copy-start.19 = (bf16[640,2048]{1,0:T(8,128)(2,1)S(1)}, bf16[640,2048]{1,0:T(8,128)(2,1)}, u32[]{:S(2)}) copy-start(bf16[640,2048]{1,0:T(8,128)(2,1)} %all-gather.26.cloned.1.call-done) | copy-start | bytes 7864324
  670.8 34.7 %copy-start.4 = (bf16[160,2048]{1,0:T(8,128)(2,1)S(1)}, bf16[160,2048]{1,0:T(8,128)(2,1)}, u32[]{:S(2)}) copy-start(bf16[160,2048]{1,0:T(8,128)(2,1)} %multiply_convert_fusion.1) | copy-start | bytes 1966084
  670.8 38.9 %copy-start.1 = (bf16[2048,32]{0,1:T(8,128)(2,1)S(1)}, bf16[2048,32]{0,1:T(8,128)(2,1)}, u32[]{:S(2)}) copy-start(bf16[2048,32]{0,1:T(8,128)(2,1)} %param.28) | copy-start | bytes 393220
  705.5 3.0 copy-start.8
  (2 other events, 4.6 us)
Sparse Core Ops, SparseCore 0:
  8.9 28.2 all-gather.9
  38.7 98.0 all-gather.11
  138.4 96.3 all-gather.13
  236.2 96.3 all-gather.15
  347.2 32.8 reduce-scatter.3
  384.5 25.5 all-gather.17
  411.6 27.9 all-gather.19
  441.2 27.3 all-gather.21
  470.2 27.3 all-gather.23
  583.9 33.8 reduce-scatter.5
  622.1 25.5 all-gather.25
  670.9 34.4 reduce-scatter.7
where the time goes:
time: 722 us; the launch traced here: 717 us
  waiting for transfers between devices  448 us (62%)
  matrix products  103 us (14%)
  other arithmetic  63.8 us (9%)
  local copies, waits for them, and re-layouts  53.9 us (7%)
  blocking collectives  33.1 us (5%)
  between operations  13.9 us (2%)
    reduce_scatter x3, waiting for transfers between devices, return_rows(): lax.psum_scatter(jnp.dot(hidden, weight_full, preferred_element_type=jnp....  102 us
    all_gather x1, waiting for transfers between devices, expand(): lax.all_gather(perceptron_switch_coefficients, 'fs', axis=0, tiled=True)  99.6 us
    all_gather x1, waiting for transfers between devices, channel_half(): lax.all_gather(perceptron_contract_coefficients, 'fs', axis=1, tiled=True)  97.8 us
    all_gather x1, waiting for transfers between devices, expand(): lax.all_gather(perceptron_expand_coefficients, 'fs', axis=0, tiled=True)  89.4 us
    all_gather x3, waiting for transfers between devices, gather_group(): return lax.all_gather(stored, 'tp', axis=0, tiled=True)  53.2 us
    dot_general x3, matrix products, return_rows(): jnp.dot(hidden, weight_full, preferred_element_type=jnp.float32)  35.1 us
    dot_general x20, matrix products, within_block(): return jnp.dot(scores, value_one, precision=highest)  30.9 us
    reduce_sum x20, other arithmetic, within_block(): jnp.sum(query_one[:, None, :] * key_one[None, :, :] * jnp.exp(spread), ax...  27.8 us
  transfers between devices with their start and end apart: 12, of which 9 were waited for; matrix products, arithmetic and copies ran while one was open for 23% of the time, Pallas kernels for 0%

commit v1 on v0

v1 whole, which is shorter than its diff:
```python
import jax
import jax.numpy as jnp
from jax import lax
from jax.experimental import pallas as pl
from jax.experimental.pallas import tpu as pltpu
from jax.sharding import PartitionSpec as P

DK = 64
DV = 128
SEQUENCE_LENGTH = 320


residual_gain = 1.681792830507429
forgetting_steepness_multiplier = 16.0
epsilon = 1e-06


def post_norm(residual, branch):
    summed = residual_gain * residual.astype(jnp.float32) + branch
    average = jnp.mean(summed, axis=-1, keepdims=True)
    centred = summed - average
    variance = jnp.mean(centred * centred, axis=-1, keepdims=True)
    return (centred * lax.rsqrt(variance + epsilon)).astype(jnp.bfloat16)


def gather_group(stored):
    return lax.all_gather(stored, "tp", axis=0, tiled=True)


def after(value, earlier):
    return lax.optimization_barrier((value, earlier))[0]


def split_gather(stored, earlier=None):
    fs_count = lax.axis_size("fs")
    grp_count = lax.axis_size("grp")
    half_rows = stored.shape[0] // grp_count
    grp = lax.axis_index("grp")
    mine = lax.dynamic_slice_in_dim(stored, grp * half_rows, half_rows, 0)
    if earlier is not None:
        mine = after(mine, earlier)
    stacked = lax.all_gather(mine, "fs", axis=0, tiled=False)
    fs = lax.axis_index("fs")
    remote = jnp.stack(
        [
            lax.dynamic_index_in_dim(stacked, lax.rem(fs + step, fs_count), 0, keepdims=False)
            for step in range(1, fs_count)
        ]
    )
    swapped = lax.ppermute(remote, "grp", [(g, (g + 1) % grp_count) for g in range(grp_count)])
    return remote, swapped


def rotated_columns(gathered):
    fs_count = lax.axis_size("fs")
    grp_count = lax.axis_size("grp")
    width = gathered.shape[1] // fs_count
    half = width // grp_count
    fs = lax.axis_index("fs")
    grp = lax.axis_index("grp")
    own = lax.dynamic_slice_in_dim(gathered, fs * width, width, 1)

    def halves(which):
        return jnp.concatenate(
            [
                lax.dynamic_slice_in_dim(
                    gathered, lax.rem(fs + step, fs_count) * width + which * half, half, 1
                )
                for step in range(1, fs_count)
            ],
            axis=1,
        )

    return own, halves(grp), halves(grp_count - 1 - grp)


def project(columns, stored, fetched):
    own, mine, other = columns
    remote, swapped = fetched
    flat = (-1, stored.shape[1])
    return (
        jnp.dot(own, stored, preferred_element_type=jnp.float32)
        + jnp.dot(mine, remote.reshape(flat), preferred_element_type=jnp.float32)
        + jnp.dot(other, swapped.reshape(flat), preferred_element_type=jnp.float32)
    )


def scatter_rows(partial):
    return lax.psum_scatter(partial, "tp", scatter_dimension=0, tiled=True)


def contract(hidden, stored, fetched, earlier):
    fs_count = lax.axis_size("fs")
    grp_count = lax.axis_size("grp")
    remote, swapped = fetched
    width = stored.shape[1]
    half = hidden.shape[1] // grp_count
    grp = lax.axis_index("grp")
    mine = lax.dynamic_slice_in_dim(hidden, grp * half, half, 1)
    other = lax.dynamic_slice_in_dim(hidden, (grp_count - 1 - grp) * half, half, 1)
    pieces = [jnp.dot(hidden, stored, preferred_element_type=jnp.float32).astype(jnp.bfloat16)]
    for step in range(fs_count - 1):
        pieces.append(
            (
                jnp.dot(mine, remote[step], preferred_element_type=jnp.float32)
                + jnp.dot(other, swapped[step], preferred_element_type=jnp.float32)
            ).astype(jnp.bfloat16)
        )
    partial = jnp.concatenate(pieces, axis=1)
    if earlier is not None:
        partial = after(partial, earlier)
    summed = scatter_rows(partial)
    fs = lax.axis_index("fs")
    ordered = [
        lax.dynamic_slice_in_dim(
            summed, lax.rem(block - fs + fs_count, fs_count) * width, width, 1
        )
        for block in range(fs_count)
    ]
    return jnp.concatenate(ordered, axis=1).astype(jnp.float32)


def mixing_kernel(head_count, projected_ref, decay_ref, gain_ref, gated_ref):
    length = projected_ref.shape[0]
    key_width = head_count * DK
    value_width = head_count * DV
    queries = projected_ref[:, :key_width].astype(jnp.float32)
    key_rows = projected_ref[:, key_width : 2 * key_width].astype(jnp.float32)
    decay = decay_ref[...]
    rows = lax.broadcasted_iota(jnp.int32, (length, length), 0)
    columns = lax.broadcasted_iota(jnp.int32, (length, length), 1)
    apart = rows ^ columns
    channel = lax.broadcasted_iota(jnp.int32, (length, key_width), 1)
    top = decay.astype(jnp.bfloat16)
    rest = decay - top.astype(jnp.float32)
    middle = rest.astype(jnp.bfloat16)
    low = (rest - middle.astype(jnp.float32)).astype(jnp.bfloat16)

    def products(query_side, key_side):
        query_side = query_side.astype(jnp.bfloat16)
        found = []
        for head in range(head_count):
            inside = (channel >= head * DK) & (channel < (head + 1) * DK)
            one = jnp.where(inside, key_side, 0.0).astype(jnp.bfloat16)
            found.append(
                lax.dot_general(
                    query_side, one, (((1,), (1,)), ((), ())), preferred_element_type=jnp.float32
                )
            )
        return found

    scores = products(queries, key_rows)
    half = 1
    while half < length:
        level = half.bit_length() - 1
        upper = (rows & half) != 0
        reach = ((rows >> level) == (columns >> level)) & (
            (upper & (columns <= rows)) | (jnp.logical_not(upper) & (columns >= rows))
        )
        reach = jnp.where(reach, 1.0, 0.0).astype(jnp.bfloat16)
        through = (
            jnp.dot(reach, top, preferred_element_type=jnp.float32)
            + jnp.dot(reach, middle, preferred_element_type=jnp.float32)
            + jnp.dot(reach, low, preferred_element_type=jnp.float32)
        )
        before = jnp.minimum(through - decay, 0.0)
        found = products(queries * jnp.exp(through), key_rows * jnp.exp(before))
        scores = [jnp.where(apart >= half, new, old) for new, old in zip(found, scores)]
        half *= 2
    for head in range(head_count):
        begin = 2 * key_width + head * DV
        values = projected_ref[:, begin : begin + DV]
        mixed = jnp.dot(
            scores[head].astype(jnp.bfloat16), values, preferred_element_type=jnp.float32
        )
        begin += value_width
        opener = projected_ref[:, begin : begin + DV].astype(jnp.float32)
        scaled = (
            mixed
            * lax.rsqrt(jnp.mean(mixed * mixed, axis=-1, keepdims=True) + epsilon)
            * gain_ref[...]
        )
        gated_ref[:, head * DV : (head + 1) * DV] = (
            scaled * (opener / (1.0 + jnp.exp(-opener)))
        ).astype(jnp.bfloat16)


def mix(projected, decay, gain):
    tokens, key_width = decay.shape
    head_count = key_width // DK
    seq_count = tokens // SEQUENCE_LENGTH

    def block(width):
        return pl.BlockSpec((SEQUENCE_LENGTH, width), lambda seq: (seq, 0))

    return pl.pallas_call(
        lambda *refs: mixing_kernel(head_count, *refs),
        out_shape=jax.ShapeDtypeStruct((tokens, head_count * DV), jnp.bfloat16),
        grid=(seq_count,),
        in_specs=[
            block(projected.shape[1]),
            block(key_width),
            pl.BlockSpec((1, DV), lambda seq: (0, 0)),
        ],
        out_specs=block(head_count * DV),
        name="mixing",
        cost_estimate=pl.CostEstimate(
            flops=4000000 * tokens, bytes_accessed=4000 * tokens, transcendentals=3000 * tokens
        ),
    )(projected, decay, gain.reshape(1, DV))


def per_device(
    incoming_representations,
    perceptron_switch_coefficients,
    perceptron_expand_coefficients,
    perceptron_contract_coefficients,
    probe_coefficients,
    address_coefficients,
    payload_coefficients,
    emit_switch_coefficients,
    forgetting_shrink_coefficients,
    forgetting_expand_coefficients,
    forgetting_sigmoid_intercept,
    extra_forgetting_logits,
    subspace_rescaling_amplitude,
    recurrence_emit_coefficients,
):
    gate_weight = split_gather(perceptron_switch_coefficients)
    up_weight = split_gather(perceptron_expand_coefficients, gate_weight[0])
    down_weight = split_gather(perceptron_contract_coefficients, up_weight[0])
    mixer_stored = jnp.concatenate(
        [
            probe_coefficients,
            address_coefficients,
            payload_coefficients,
            emit_switch_coefficients,
        ],
        axis=1,
    )
    mixer_weight = split_gather(mixer_stored, down_weight[0])
    out_full = lax.all_gather(recurrence_emit_coefficients, "fs", axis=1, tiled=True)

    def channel_half(stored, entry, earlier):
        columns = rotated_columns(gather_group(entry))
        gate_sum = project(columns, perceptron_switch_coefficients, gate_weight)
        up_sum = project(columns, perceptron_expand_coefficients, up_weight)
        hidden = (jax.nn.silu(gate_sum) * up_sum).astype(jnp.bfloat16)
        return post_norm(
            stored, 0.5 * contract(hidden, perceptron_contract_coefficients, down_weight, earlier)
        )

    opening_perceptron_result = channel_half(
        incoming_representations,
        after(incoming_representations, up_weight[0]),
        mixer_weight[0],
    )
    gathered = gather_group(opening_perceptron_result)
    projected = project(rotated_columns(gathered), mixer_stored, mixer_weight).astype(
        jnp.bfloat16
    )
    compact_inner_dimensionality = jnp.dot(
        gathered, forgetting_shrink_coefficients, preferred_element_type=jnp.float32
    ).astype(jnp.bfloat16)
    forgetting_euler_power = (
        jax.nn.log_sigmoid(
            jnp.dot(
                compact_inner_dimensionality,
                forgetting_expand_coefficients,
                preferred_element_type=jnp.float32,
            )
            + forgetting_sigmoid_intercept
        )
        / forgetting_steepness_multiplier
        + extra_forgetting_logits
    )
    gated = mix(projected, forgetting_euler_power, subspace_rescaling_amplitude)
    branch = scatter_rows(
        jnp.dot(gated, out_full, preferred_element_type=jnp.float32).astype(jnp.bfloat16)
    ).astype(jnp.float32)
    context_blend_result = post_norm(opening_perceptron_result, branch)
    return channel_half(context_blend_result, context_blend_result, None)


def solution(mesh):
    return jax.shard_map(
        per_device,
        mesh=mesh,
        in_specs=(
            P(("grp", "fs", "tp"), None),
            P("fs", "tp"),
            P("fs", "tp"),
            P("tp", "fs"),
            P("fs", "tp"),
            P("fs", "tp"),
            P("fs", "tp"),
            P("fs", "tp"),
            P(),
            P(None, "tp"),
            P("tp"),
            P(("grp", "fs"), "tp"),
            P(),
            P("tp", "fs"),
        ),
        out_specs=P(("grp", "fs", "tp"), None),
        check_vma=False,
    )
```

time: 722 us -> 524 us (0.73)
  waiting for transfers between devices: 448 us -> 365 us
  matrix products: 103 us -> 65.2 us
  other arithmetic: 63.8 us -> 28.6 us
  blocking collectives: 33.1 us -> 0 us
  local copies, waits for them, and re-layouts: 53.9 us -> 30.3 us
  Pallas kernels: 0 us -> 11.5 us
    all_gather x5 -> x4, waiting for transfers between devices: 288 us -> 158 us  [split_gather(): stacked = lax.all_gather(mine, 'fs', axis=0, tiled=False)]
    dot_general x32 -> x30, matrix products: 99.7 us -> 61.4 us  [the longest x5 17.2 us: project(): jnp.dot(other, swapped.reshape(flat), preferred_element_type=jnp.float32)]
    all_gather x2 -> x0, blocking collectives: 33.1 us -> none  [the longest x1 17.1 us: per_device(): lax.all_gather(probe_coefficients, 'fs', axis=0, tiled=True)]
    ppermute x0 -> x4, waiting for transfers between devices: none -> 31.9 us  [split_gather(): lax.ppermute(remote, 'grp', [(g, (g + 1) % grp_count) for g in range(grp_...]
    reduce_sum x20 -> x0, other arithmetic: 27.8 us -> none  [within_block(): jnp.sum(query_one[:, None, :] * key_one[None, :, :] * jnp.exp(spread), ax...]
    mul x32 -> x0, local copies, waits for them, and re-layouts: 21 us -> none  [the longest x20 15.6 us: within_block(): query_one[:, None, :] * key_one[None, :, :] * jnp.exp(spread)]
    dynamic_slice x0 -> x13, local copies, waits for them, and re-layouts: none -> 17.7 us  [the longest x4 6.13 us: split_gather(): lax.dynamic_index_in_dim(stacked, lax.rem(fs + step, fs_count), 0, keepdi...]
    all_gather x3, waiting for transfers between devices: 53.2 us -> 70 us  [gather_group(): return lax.all_gather(stored, 'tp', axis=0, tiled=True)]
  transfers between devices with their start and end apart: 12 -> 15, of which waited for: 9 -> 11; matrix products, arithmetic and copies ran while one was open for 23% -> 11% of each run, Pallas kernels for 0% -> 2%
where the time goes in v1:
time: 524 us; the launch traced here: 521 us
  waiting for transfers between devices  365 us (70%)
  matrix products  65.2 us (12%)
  local copies, waits for them, and re-layouts  30.3 us (6%)
  other arithmetic  28.6 us (5%)
  between operations  14.1 us (3%)
  Pallas kernels  11.5 us (2%)
  starting transfers between devices  6.17 us (1%)
    all_gather x4, waiting for transfers between devices, split_gather(): stacked = lax.all_gather(mine, 'fs', axis=0, tiled=False)  158 us
    reduce_scatter x3, waiting for transfers between devices, scatter_rows(): return lax.psum_scatter(partial, 'tp', scatter_dimension=0, tiled=True)  102 us
    all_gather x3, waiting for transfers between devices, gather_group(): return lax.all_gather(stored, 'tp', axis=0, tiled=True)  70 us
    ppermute x4, waiting for transfers between devices, split_gather(): lax.ppermute(remote, 'grp', [(g, (g + 1) % grp_count) for g in range(grp_...  31.9 us
    dot_general x5, matrix products, project(): jnp.dot(other, swapped.reshape(flat), preferred_element_type=jnp.float32)  17.2 us
    concatenate x2, other arithmetic, contract(): partial = jnp.concatenate(pieces, axis=1)  14.9 us
    dot_general x5, matrix products, project(): jnp.dot(mine, remote.reshape(flat), preferred_element_type=jnp.float32)  14.5 us
    unnamed x59, local copies, waits for them, and re-layouts  12.6 us
  transfers between devices with their start and end apart: 15, of which 11 were waited for; matrix products, arithmetic and copies ran while one was open for 11% of the time, Pallas kernels for 2%

profile of v1, /device:TPU:0, one launch (start us, length us, event | category | flops | bytes accessed | tf_op | source)
XLA Modules:
  0.0 520.8 jit_solution(12833374511461142557)
XLA Ops:
  9.7 56.7 %all-gather.21.cloned.1.call-done = bf16[1024,1280]{1,0:T(8,128)(2,1)} async-done(((bf16[256,1280]{1,0:T(8,128)(2,1)}), bf16[1024,1280]{1,0:T(8,128)(2,1)}) %all-gather.21.cloned.1.call-update) | async-done | bytes 2621456 | tf_op jit(solution)/shard_map/all_gather | solution.py:42
  70.6 52.7 %all-gather.23.cloned.1.call-done = bf16[1024,1280]{1,0:T(8,128)(2,1)} async-done(((bf16[256,1280]{1,0:T(8,128)(2,1)}), bf16[1024,1280]{1,0:T(8,128)(2,1)}) %all-gather.23.cloned.1.call-update) | async-done | bytes 2621456 | tf_op jit(solution)/shard_map/all_gather | solution.py:42
  131.0 49.0 %all-gather.25.cloned.1.call-done = bf16[2560,512]{1,0:T(8,128)(2,1)} async-done(((bf16[640,512]{1,0:T(8,128)(2,1)}), bf16[2560,512]{1,0:T(8,128)(2,1)}) %all-gather.25.cloned.1.call-update) | async-done | bytes 2621456 | tf_op jit(solution)/shard_map/all_gather | solution.py:42
  185.3 20.6 %all-gather.13.cloned.1.call-done = bf16[640,2048]{1,0:T(8,128)(2,1)} async-done(((bf16[160,2048]{1,0:T(8,128)(2,1)}), bf16[640,2048]{1,0:T(8,128)(2,1)}) %all-gather.13.cloned.1.call-update) | async-done | bytes 2621456 | tf_op jit(solution)/shard_map/all_gather | solution.py:27
  207.4 3.0 fusion.57
  210.5 3.1 fusion.58
  215.7 3.0 convolution_add_fusion.7
  218.7 3.2 fusion.2
  226.1 31.9 %collective-permute-done.2 = bf16[3,640,512]{2,1,0:T(8,128)(2,1)} collective-permute-done((bf16[3,640,512]{2,1,0:T(8,128)(2,1)}, bf16[3,640,512]{2,1,0:T(8,128)(2,1)}, u32[]{:S(2)}, u32[]{:S(2)}) %collective-permute-start.2) | collective-permute-done | bytes 1966112 | tf_op jit(solution)/shard_map/ppermute | solution.py:50
  259.9 1.9 fusion.5
  263.8 7.4 %pad_maximum_fusion = bf16[640,2048]{0,1:T(8,128)(2,1)} fusion(bf16[640,512]{0,1:T(8,128)(2,1)S(1)} %fusion.6, bf16[640,512]{0,1:T(8,128)(2,1)S(1)} %fusion.5, bf16[640,512]{0,1:T(8,128)(2,1)S(1)} %fusion.4, bf16[640,512]{0,1:T(8,128)(2,1)S(1)} %convolution_convert_fusion.2), kind=kLoop, calls=%fused_computation.13 | loop fusion | flops 10485760 | bytes 5242880 | tf_op jit(solution)/shard_map/concatenate | solution.py:109
  273.6 4.5 copy.33
  278.3 33.5 %reduce-scatter.10.cloned.1.call-done = bf16[160,2048]{1,0:T(8,128)(2,1)} async-done(((bf16[640,2048]{1,0:T(8,128)(2,1)}), bf16[160,2048]{1,0:T(8,128)(2,1)}) %reduce-scatter.10.cloned.1.call-update) | async-done | bytes 655376 | tf_op jit(solution)/shard_map/reduce_scatter | solution.py:89
  316.6 24.0 %all-gather.15.cloned.1.call-done = bf16[640,2048]{1,0:T(8,128)(2,1)} async-done(((bf16[160,2048]{1,0:T(8,128)(2,1)}), bf16[640,2048]{1,0:T(8,128)(2,1)}) %all-gather.15.cloned.1.call-update) | async-done | bytes 2621456 | tf_op jit(solution)/shard_map/all_gather | solution.py:27
  340.7 2.5 constant_dynamic-slice_fusion.12
  343.2 3.1 fusion.37
  346.4 2.3 fusion.12
  348.6 3.8 fusion.61.refs_1_
  352.4 4.6 add_convert_fusion.refs_0_
  357.0 11.5 %mixing.1 = bf16[640,256]{1,0:T(8,128)(2,1)} custom-call(bf16[640,768]{1,0:T(8,128)(2,1)} %add_convert_fusion.refs_0_, f32[640,128]{1,0:T(8,128)} %fusion.61.refs_1_, f32[1,128]{1,0:T(1,128)} %bitcast.70), custom_call_target="tpu_custom_call" | custom-call | flops 2560000000 | bytes 2560000 | tf_op jit(solution)/shard_map/mixing/pallas_call | solution.py:196
  370.3 3.7 convolution_convert_fusion
  374.0 34.0 %reduce-scatter.12.cloned.1.call-done = bf16[160,2048]{1,0:T(8,128)(2,1)} async-done(((bf16[640,2048]{1,0:T(8,128)(2,1)}), bf16[160,2048]{1,0:T(8,128)(2,1)}) %reduce-scatter.12.cloned.1.call-update) | async-done | bytes 655376 | tf_op jit(solution)/shard_map/reduce_scatter | solution.py:89
  412.3 25.4 %all-gather.19.cloned.1.call-done = bf16[640,2048]{1,0:T(8,128)(2,1)} async-done(((bf16[160,2048]{1,0:T(8,128)(2,1)}), bf16[640,2048]{1,0:T(8,128)(2,1)}) %all-gather.19.cloned.1.call-update) | async-done | bytes 2621456 | tf_op jit(solution)/shard_map/all_gather | solution.py:27
  439.4 3.0 fusion.55
  442.4 3.1 fusion.56
  446.6 3.1 convolution_add_fusion.5
  450.8 3.3 fusion.3
  458.3 1.9 fusion.9
  460.3 1.9 fusion.8
  464.1 7.5 %pad_maximum_fusion.1 = bf16[640,2048]{0,1:T(8,128)(2,1)} fusion(bf16[640,512]{0,1:T(8,128)(2,1)S(1)} %fusion.9, bf16[640,512]{0,1:T(8,128)(2,1)S(1)} %fusion.8, bf16[640,512]{0,1:T(8,128)(2,1)S(1)} %fusion.7, bf16[640,512]{0,1:T(8,128)(2,1)S(1)} %convolution_convert_fusion.1), kind=kLoop, calls=%fused_computation.14 | loop fusion | flops 10485760 | bytes 5242880 | tf_op jit(solution)/shard_map/concatenate | solution.py:109
  471.6 4.5 copy.37
  476.2 34.6 %reduce-scatter.14.cloned.1.call-done = bf16[160,2048]{1,0:T(8,128)(2,1)} async-done(((bf16[640,2048]{1,0:T(8,128)(2,1)}), bf16[160,2048]{1,0:T(8,128)(2,1)}) %reduce-scatter.14.cloned.1.call-update) | async-done | bytes 655376 | tf_op jit(solution)/shard_map/reduce_scatter | solution.py:89
  (135 shorter events, 58.3 us)
Async XLA Ops:
  6.5 2.3 copy-start.6
  6.5 59.9 %all-gather.21.cloned.1.call-start = ((), (), s32[]{:S(2)}) async-start(), calls=%async_computation.7 | async-start | bytes 3276800 | tf_op jit(solution)/shard_map/all_gather | solution.py:42
  8.8 114.5 %all-gather.23.cloned.1.call-start = ((), (), s32[]{:S(2)}) async-start(), calls=%async_computation.8 | async-start | bytes 3276800 | tf_op jit(solution)/shard_map/all_gather | solution.py:42
  69.6 110.5 %all-gather.25.cloned.1.call-start = ((), (), s32[]{:S(2)}) async-start(), calls=%async_computation.9 | async-start | bytes 3276800 | tf_op jit(solution)/shard_map/all_gather | solution.py:42
  124.9 2.3 copy-start.20
  126.4 79.4 %all-gather.13.cloned.1.call-start = ((), (), s32[]{:S(2)}) async-start(), calls=%async_computation.3 | async-start | bytes 3276800 | tf_op jit(solution)/shard_map/all_gather | solution.py:27
  127.0 144.2 %all-gather.27.cloned.1.call-start = ((), (), s32[]{:S(2)}) async-start(), calls=%async_computation.10 | async-start | bytes 1966080 | tf_op jit(solution)/shard_map/all_gather | solution.py:42
  129.0 86.7 %collective-permute-start = (bf16[3,256,1280]{2,1,0:T(8,128)(2,1)}, bf16[3,256,1280]{2,1,0:T(8,128)(2,1)}, u32[]{:S(2)}, u32[]{:S(2)}) collective-permute-start(bf16[3,256,1280]{2,1,0:T(8,128)(2,1)} %pad_maximum_fusion.2), channel_id=1, source_target_pairs={{0,16},{16,0},{1,17},{17,1},{2,18},{18,2},{3,19},{19,3},{4,20},{20... | collective-permute-start | bytes 5898248 | tf_op jit(solution)/shard_map/ppermute | solution.py:50
  130.5 88.2 %collective-permute-start.1 = (bf16[3,256,1280]{2,1,0:T(8,128)(2,1)}, bf16[3,256,1280]{2,1,0:T(8,128)(2,1)}, u32[]{:S(2)}, u32[]{:S(2)}) collective-permute-start(bf16[3,256,1280]{2,1,0:T(8,128)(2,1)} %pad_maximum_fusion.3), channel_id=1, source_target_pairs={{0,16},{16,0},{1,17},{17,1},{2,18},{18,2},{3,19},{19,3},{4,20},{20... | collective-permute-start | bytes 5898248 | tf_op jit(solution)/shard_map/ppermute | solution.py:50
  181.7 40.2 %copy-start.4 = (bf16[1,640,512]{2,1,0:T(8,128)(2,1)}, bf16[1,640,512]{2,1,0:T(8,128)(2,1)S(1)}, u32[]{:S(2)}) copy-start(bf16[1,640,512]{2,1,0:T(8,128)(2,1)S(1)} %get-tuple-element.28) | copy-start | bytes 1966084
  183.2 74.8 %collective-permute-start.2 = (bf16[3,640,512]{2,1,0:T(8,128)(2,1)}, bf16[3,640,512]{2,1,0:T(8,128)(2,1)}, u32[]{:S(2)}, u32[]{:S(2)}) collective-permute-start(bf16[3,640,512]{2,1,0:T(8,128)(2,1)} %pad_maximum_fusion.4), channel_id=1, source_target_pairs={{0,16},{16,0},{1,17},{17,1},{2,18},{18,2},{3,19},{19,3},{4,20},{20... | collective-permute-start | bytes 5898248 | tf_op jit(solution)/shard_map/ppermute | solution.py:50
  184.7 127.1 %reduce-scatter.10.cloned.1.call-start = ((), (), s32[]{:S(2)}) async-start(), calls=%async_computation.11 | async-start | bytes 3276800 | tf_op jit(solution)/shard_map/reduce_scatter | solution.py:89
  210.4 3.2 copy-start.7
  210.5 3.2 copy-start.10
  278.2 34.8 %copy-start.3 = (bf16[160,2048]{1,0:T(8,128)(2,1)S(1)}, bf16[160,2048]{1,0:T(8,128)(2,1)}, u32[]{:S(2)}) copy-start(bf16[160,2048]{1,0:T(8,128)(2,1)} %param.14) | copy-start | bytes 1966084
  278.2 62.5 %all-gather.15.cloned.1.call-start = ((), (), s32[]{:S(2)}) async-start(), calls=%async_computation.4 | async-start | bytes 3276800 | tf_op jit(solution)/shard_map/all_gather | solution.py:27
  315.0 55.3 %all-gather.17.cloned.1.call-start = ((), (), s32[]{:S(2)}) async-start(), calls=%async_computation.5 | async-start | bytes 1310720 | tf_op jit(solution)/shard_map/all_gather | solution.py:242
  315.0 37.4 %collective-permute-start.3 = (bf16[3,256,768]{2,1,0:T(8,128)(2,1)}, bf16[3,256,768]{2,1,0:T(8,128)(2,1)}, u32[]{:S(2)}, u32[]{:S(2)}) collective-permute-start(bf16[3,256,768]{2,1,0:T(8,128)(2,1)} %pad_maximum_fusion.5), channel_id=1, source_target_pairs={{0,16},{16,0},{1,17},{17,1},{2,18},{18,2},{3,19},{19,3},{4,20},{20... | collective-permute-start | bytes 3538952 | tf_op jit(solution)/shard_map/ppermute | solution.py:50
  316.6 26.6 %copy-start.13 = (bf16[512,768]{1,0:T(8,128)(2,1)S(1)}, bf16[512,768]{1,0:T(8,128)(2,1)}, u32[]{:S(2)}) copy-start(bf16[512,768]{1,0:T(8,128)(2,1)} %copy-done.12) | copy-start | bytes 2359300
  316.6 91.4 %reduce-scatter.12.cloned.1.call-start = ((), (), s32[]{:S(2)}) async-start(), calls=%async_computation.12 | async-start | bytes 3276800 | tf_op jit(solution)/shard_map/reduce_scatter | solution.py:89
  343.2 3.1 copy-start.16
  346.3 2.3 copy-start.26
  348.6 3.8 copy-start.14
  348.6 3.8 copy-start.15
  373.9 34.1 %copy-start.2 = (bf16[160,2048]{1,0:T(8,128)(2,1)S(1)}, bf16[160,2048]{1,0:T(8,128)(2,1)}, u32[]{:S(2)}) copy-start(bf16[160,2048]{1,0:T(8,128)(2,1)} %multiply_convert_fusion.2) | copy-start | bytes 1966084
  373.9 63.8 %all-gather.19.cloned.1.call-start = ((), (), s32[]{:S(2)}) async-start(), calls=%async_computation.6 | async-start | bytes 3276800 | tf_op jit(solution)/shard_map/all_gather | solution.py:27
  408.0 2.9 copy-start.9
  412.1 98.7 %reduce-scatter.14.cloned.1.call-start = ((), (), s32[]{:S(2)}) async-start(), calls=%async_computation.13 | async-start | bytes 3276800 | tf_op jit(solution)/shard_map/reduce_scatter | solution.py:89
  442.4 3.2 copy-start.11
  446.6 3.1 copy-start.8
  450.8 3.4 copy-start.5
  476.2 35.9 %copy-start.1 = (bf16[160,2048]{1,0:T(8,128)(2,1)S(1)}, bf16[160,2048]{1,0:T(8,128)(2,1)}, u32[]{:S(2)}) copy-start(bf16[160,2048]{1,0:T(8,128)(2,1)} %multiply_convert_fusion.1) | copy-start | bytes 1966084
  (10 other events, 16.5 us)
Sparse Core Ops, SparseCore 0:
  8.9 57.4 all-gather.20
  69.7 53.5 all-gather.22
  126.5 53.5 all-gather.24
  181.5 24.2 all-gather.12
  207.2 37.0 all-gather.26
  278.3 33.4 reduce-scatter.9
  315.1 25.5 all-gather.14
  342.2 27.9 all-gather.16
  374.1 33.8 reduce-scatter.11
  412.2 25.5 all-gather.18
  476.3 34.4 reduce-scatter.13

commit v2 on v1

--- a/solution.py
+++ b/solution.py
@@ -2,7 +2,6 @@
 import jax.numpy as jnp
 from jax import lax
 from jax.experimental import pallas as pl
-from jax.experimental.pallas import tpu as pltpu
 from jax.sharding import PartitionSpec as P
 
 DK = 64
@@ -47,7 +46,9 @@
             for step in range(1, fs_count)
         ]
     )
-    swapped = lax.ppermute(remote, "grp", [(g, (g + 1) % grp_count) for g in range(grp_count)])
+    swapped = lax.ppermute(
+        remote, "grp", [(g, (g + 1) % grp_count) for g in range(grp_count)]
+    )
     return remote, swapped
 
 
@@ -242,7 +243,8 @@
     out_full = lax.all_gather(recurrence_emit_coefficients, "fs", axis=1, tiled=True)
 
     def channel_half(stored, entry, earlier):
-        columns = rotated_columns(gather_group(entry))
+        gathered = gather_group(entry)
+        columns = rotated_columns(gathered)
         gate_sum = project(columns, perceptron_switch_coefficients, gate_weight)
         up_sum = project(columns, perceptron_expand_coefficients, up_weight)
         hidden = (jax.nn.silu(gate_sum) * up_sum).astype(jnp.bfloat16)

time: 524 us -> 524 us (level)
  no operation moved by 1% of the time
where the time goes in v2:
time: 524 us; the launch traced here: 521 us
  waiting for transfers between devices  365 us (70%)
  matrix products  65.2 us (12%)
  local copies, waits for them, and re-layouts  30.3 us (6%)
  other arithmetic  28.6 us (5%)
  between operations  14.1 us (3%)
  Pallas kernels  11.5 us (2%)
  starting transfers between devices  6.17 us (1%)
    all_gather x4, waiting for transfers between devices, split_gather(): stacked = lax.all_gather(mine, 'fs', axis=0, tiled=False)  158 us
    reduce_scatter x3, waiting for transfers between devices, scatter_rows(): return lax.psum_scatter(partial, 'tp', scatter_dimension=0, tiled=True)  102 us
    all_gather x3, waiting for transfers between devices, gather_group(): return lax.all_gather(stored, 'tp', axis=0, tiled=True)  70 us
    ppermute x4, waiting for transfers between devices, split_gather(): lax.ppermute(remote, 'grp', [(g, (g + 1) % grp_count) for g in range(grp_...  31.9 us
    dot_general x5, matrix products, project(): jnp.dot(other, swapped.reshape(flat), preferred_element_type=jnp.float32)  17.2 us
    concatenate x2, other arithmetic, contract(): partial = jnp.concatenate(pieces, axis=1)  14.9 us
    dot_general x5, matrix products, project(): jnp.dot(mine, remote.reshape(flat), preferred_element_type=jnp.float32)  14.5 us
    unnamed x59, local copies, waits for them, and re-layouts  12.6 us
  transfers between devices with their start and end apart: 15, of which 11 were waited for; matrix products, arithmetic and copies ran while one was open for 11% of the time, Pallas kernels for 2%

profile of v2, /device:TPU:0, one launch (start us, length us, event | category | flops | bytes accessed | tf_op | source)
XLA Modules:
  0.0 520.8 jit_solution(12833374511461142557)
XLA Ops:
  9.7 56.7 %all-gather.21.cloned.1.call-done = bf16[1024,1280]{1,0:T(8,128)(2,1)} async-done(((bf16[256,1280]{1,0:T(8,128)(2,1)}), bf16[1024,1280]{1,0:T(8,128)(2,1)}) %all-gather.21.cloned.1.call-update) | async-done | bytes 2621456 | tf_op jit(solution)/shard_map/all_gather | solution.py:41
  70.6 52.7 %all-gather.23.cloned.1.call-done = bf16[1024,1280]{1,0:T(8,128)(2,1)} async-done(((bf16[256,1280]{1,0:T(8,128)(2,1)}), bf16[1024,1280]{1,0:T(8,128)(2,1)}) %all-gather.23.cloned.1.call-update) | async-done | bytes 2621456 | tf_op jit(solution)/shard_map/all_gather | solution.py:41
  131.0 49.0 %all-gather.25.cloned.1.call-done = bf16[2560,512]{1,0:T(8,128)(2,1)} async-done(((bf16[640,512]{1,0:T(8,128)(2,1)}), bf16[2560,512]{1,0:T(8,128)(2,1)}) %all-gather.25.cloned.1.call-update) | async-done | bytes 2621456 | tf_op jit(solution)/shard_map/all_gather | solution.py:41
  185.3 20.6 %all-gather.13.cloned.1.call-done = bf16[640,2048]{1,0:T(8,128)(2,1)} async-done(((bf16[160,2048]{1,0:T(8,128)(2,1)}), bf16[640,2048]{1,0:T(8,128)(2,1)}) %all-gather.13.cloned.1.call-update) | async-done | bytes 2621456 | tf_op jit(solution)/shard_map/all_gather | solution.py:26
  207.4 3.0 fusion.57
  210.5 3.1 fusion.58
  215.7 3.0 convolution_add_fusion.7
  218.7 3.2 fusion.2
  226.1 31.9 %collective-permute-done.2 = bf16[3,640,512]{2,1,0:T(8,128)(2,1)} collective-permute-done((bf16[3,640,512]{2,1,0:T(8,128)(2,1)}, bf16[3,640,512]{2,1,0:T(8,128)(2,1)}, u32[]{:S(2)}, u32[]{:S(2)}) %collective-permute-start.2) | collective-permute-done | bytes 1966112 | tf_op jit(solution)/shard_map/ppermute | solution.py:49
  259.9 1.9 fusion.5
  263.8 7.4 %pad_maximum_fusion = bf16[640,2048]{0,1:T(8,128)(2,1)} fusion(bf16[640,512]{0,1:T(8,128)(2,1)S(1)} %fusion.6, bf16[640,512]{0,1:T(8,128)(2,1)S(1)} %fusion.5, bf16[640,512]{0,1:T(8,128)(2,1)S(1)} %fusion.4, bf16[640,512]{0,1:T(8,128)(2,1)S(1)} %convolution_convert_fusion.2), kind=kLoop, calls=%fused_computation.13 | loop fusion | flops 10485760 | bytes 5242880 | tf_op jit(solution)/shard_map/concatenate | solution.py:110
  273.6 4.5 copy.33
  278.3 33.5 %reduce-scatter.10.cloned.1.call-done = bf16[160,2048]{1,0:T(8,128)(2,1)} async-done(((bf16[640,2048]{1,0:T(8,128)(2,1)}), bf16[160,2048]{1,0:T(8,128)(2,1)}) %reduce-scatter.10.cloned.1.call-update) | async-done | bytes 655376 | tf_op jit(solution)/shard_map/reduce_scatter | solution.py:90
  316.6 24.0 %all-gather.15.cloned.1.call-done = bf16[640,2048]{1,0:T(8,128)(2,1)} async-done(((bf16[160,2048]{1,0:T(8,128)(2,1)}), bf16[640,2048]{1,0:T(8,128)(2,1)}) %all-gather.15.cloned.1.call-update) | async-done | bytes 2621456 | tf_op jit(solution)/shard_map/all_gather | solution.py:26
  340.7 2.5 constant_dynamic-slice_fusion.12
  343.2 3.1 fusion.37
  346.4 2.3 fusion.12
  348.6 3.8 fusion.61.refs_1_
  352.4 4.6 add_convert_fusion.refs_0_
  357.0 11.5 %mixing.1 = bf16[640,256]{1,0:T(8,128)(2,1)} custom-call(bf16[640,768]{1,0:T(8,128)(2,1)} %add_convert_fusion.refs_0_, f32[640,128]{1,0:T(8,128)} %fusion.61.refs_1_, f32[1,128]{1,0:T(1,128)} %bitcast.70), custom_call_target="tpu_custom_call" | custom-call | flops 2560000000 | bytes 2560000 | tf_op jit(solution)/shard_map/mixing/pallas_call | solution.py:197
  370.3 3.7 convolution_convert_fusion
  374.0 34.0 %reduce-scatter.12.cloned.1.call-done = bf16[160,2048]{1,0:T(8,128)(2,1)} async-done(((bf16[640,2048]{1,0:T(8,128)(2,1)}), bf16[160,2048]{1,0:T(8,128)(2,1)}) %reduce-scatter.12.cloned.1.call-update) | async-done | bytes 655376 | tf_op jit(solution)/shard_map/reduce_scatter | solution.py:90
  412.3 25.4 %all-gather.19.cloned.1.call-done = bf16[640,2048]{1,0:T(8,128)(2,1)} async-done(((bf16[160,2048]{1,0:T(8,128)(2,1)}), bf16[640,2048]{1,0:T(8,128)(2,1)}) %all-gather.19.cloned.1.call-update) | async-done | bytes 2621456 | tf_op jit(solution)/shard_map/all_gather | solution.py:26
  439.4 3.0 fusion.55
  442.4 3.1 fusion.56
  446.6 3.1 convolution_add_fusion.5
  450.8 3.3 fusion.3
  458.3 1.9 fusion.9
  462.2 1.9 fusion.7
  464.1 7.5 %pad_maximum_fusion.1 = bf16[640,2048]{0,1:T(8,128)(2,1)} fusion(bf16[640,512]{0,1:T(8,128)(2,1)S(1)} %fusion.9, bf16[640,512]{0,1:T(8,128)(2,1)S(1)} %fusion.8, bf16[640,512]{0,1:T(8,128)(2,1)S(1)} %fusion.7, bf16[640,512]{0,1:T(8,128)(2,1)S(1)} %convolution_convert_fusion.1), kind=kLoop, calls=%fused_computation.14 | loop fusion | flops 10485760 | bytes 5242880 | tf_op jit(solution)/shard_map/concatenate | solution.py:110
  471.6 4.5 copy.37
  476.2 34.6 %reduce-scatter.14.cloned.1.call-done = bf16[160,2048]{1,0:T(8,128)(2,1)} async-done(((bf16[640,2048]{1,0:T(8,128)(2,1)}), bf16[160,2048]{1,0:T(8,128)(2,1)}) %reduce-scatter.14.cloned.1.call-update) | async-done | bytes 655376 | tf_op jit(solution)/shard_map/reduce_scatter | solution.py:90
  (135 shorter events, 58.3 us)
Async XLA Ops:
  6.5 2.3 copy-start.6
  6.5 59.9 %all-gather.21.cloned.1.call-start = ((), (), s32[]{:S(2)}) async-start(), calls=%async_computation.7 | async-start | bytes 3276800 | tf_op jit(solution)/shard_map/all_gather | solution.py:41
  8.8 114.5 %all-gather.23.cloned.1.call-start = ((), (), s32[]{:S(2)}) async-start(), calls=%async_computation.8 | async-start | bytes 3276800 | tf_op jit(solution)/shard_map/all_gather | solution.py:41
  69.6 110.5 %all-gather.25.cloned.1.call-start = ((), (), s32[]{:S(2)}) async-start(), calls=%async_computation.9 | async-start | bytes 3276800 | tf_op jit(solution)/shard_map/all_gather | solution.py:41
  124.9 2.3 copy-start.20
  126.4 79.4 %all-gather.13.cloned.1.call-start = ((), (), s32[]{:S(2)}) async-start(), calls=%async_computation.3 | async-start | bytes 3276800 | tf_op jit(solution)/shard_map/all_gather | solution.py:26
  127.0 144.2 %all-gather.27.cloned.1.call-start = ((), (), s32[]{:S(2)}) async-start(), calls=%async_computation.10 | async-start | bytes 1966080 | tf_op jit(solution)/shard_map/all_gather | solution.py:41
  129.0 86.7 %collective-permute-start = (bf16[3,256,1280]{2,1,0:T(8,128)(2,1)}, bf16[3,256,1280]{2,1,0:T(8,128)(2,1)}, u32[]{:S(2)}, u32[]{:S(2)}) collective-permute-start(bf16[3,256,1280]{2,1,0:T(8,128)(2,1)} %pad_maximum_fusion.2), channel_id=1, source_target_pairs={{0,16},{16,0},{1,17},{17,1},{2,18},{18,2},{3,19},{19,3},{4,20},{20... | collective-permute-start | bytes 5898248 | tf_op jit(solution)/shard_map/ppermute | solution.py:49
  130.5 88.2 %collective-permute-start.1 = (bf16[3,256,1280]{2,1,0:T(8,128)(2,1)}, bf16[3,256,1280]{2,1,0:T(8,128)(2,1)}, u32[]{:S(2)}, u32[]{:S(2)}) collective-permute-start(bf16[3,256,1280]{2,1,0:T(8,128)(2,1)} %pad_maximum_fusion.3), channel_id=1, source_target_pairs={{0,16},{16,0},{1,17},{17,1},{2,18},{18,2},{3,19},{19,3},{4,20},{20... | collective-permute-start | bytes 5898248 | tf_op jit(solution)/shard_map/ppermute | solution.py:49
  181.7 40.2 %copy-start.4 = (bf16[1,640,512]{2,1,0:T(8,128)(2,1)}, bf16[1,640,512]{2,1,0:T(8,128)(2,1)S(1)}, u32[]{:S(2)}) copy-start(bf16[1,640,512]{2,1,0:T(8,128)(2,1)S(1)} %get-tuple-element.28) | copy-start | bytes 1966084
  183.2 74.8 %collective-permute-start.2 = (bf16[3,640,512]{2,1,0:T(8,128)(2,1)}, bf16[3,640,512]{2,1,0:T(8,128)(2,1)}, u32[]{:S(2)}, u32[]{:S(2)}) collective-permute-start(bf16[3,640,512]{2,1,0:T(8,128)(2,1)} %pad_maximum_fusion.4), channel_id=1, source_target_pairs={{0,16},{16,0},{1,17},{17,1},{2,18},{18,2},{3,19},{19,3},{4,20},{20... | collective-permute-start | bytes 5898248 | tf_op jit(solution)/shard_map/ppermute | solution.py:49
  184.7 127.1 %reduce-scatter.10.cloned.1.call-start = ((), (), s32[]{:S(2)}) async-start(), calls=%async_computation.11 | async-start | bytes 3276800 | tf_op jit(solution)/shard_map/reduce_scatter | solution.py:90
  210.4 3.2 copy-start.7
  210.5 3.2 copy-start.10
  278.2 34.8 %copy-start.3 = (bf16[160,2048]{1,0:T(8,128)(2,1)S(1)}, bf16[160,2048]{1,0:T(8,128)(2,1)}, u32[]{:S(2)}) copy-start(bf16[160,2048]{1,0:T(8,128)(2,1)} %param.14) | copy-start | bytes 1966084
  278.2 62.5 %all-gather.15.cloned.1.call-start = ((), (), s32[]{:S(2)}) async-start(), calls=%async_computation.4 | async-start | bytes 3276800 | tf_op jit(solution)/shard_map/all_gather | solution.py:26
  315.0 55.3 %all-gather.17.cloned.1.call-start = ((), (), s32[]{:S(2)}) async-start(), calls=%async_computation.5 | async-start | bytes 1310720 | tf_op jit(solution)/shard_map/all_gather | solution.py:243
  315.0 37.4 %collective-permute-start.3 = (bf16[3,256,768]{2,1,0:T(8,128)(2,1)}, bf16[3,256,768]{2,1,0:T(8,128)(2,1)}, u32[]{:S(2)}, u32[]{:S(2)}) collective-permute-start(bf16[3,256,768]{2,1,0:T(8,128)(2,1)} %pad_maximum_fusion.5), channel_id=1, source_target_pairs={{0,16},{16,0},{1,17},{17,1},{2,18},{18,2},{3,19},{19,3},{4,20},{20... | collective-permute-start | bytes 3538952 | tf_op jit(solution)/shard_map/ppermute | solution.py:49
  316.6 26.6 %copy-start.13 = (bf16[512,768]{1,0:T(8,128)(2,1)S(1)}, bf16[512,768]{1,0:T(8,128)(2,1)}, u32[]{:S(2)}) copy-start(bf16[512,768]{1,0:T(8,128)(2,1)} %copy-done.12) | copy-start | bytes 2359300
  316.6 91.4 %reduce-scatter.12.cloned.1.call-start = ((), (), s32[]{:S(2)}) async-start(), calls=%async_computation.12 | async-start | bytes 3276800 | tf_op jit(solution)/shard_map/reduce_scatter | solution.py:90
  343.2 3.1 copy-start.16
  346.3 2.3 copy-start.26
  348.6 3.8 copy-start.14
  348.6 3.8 copy-start.15
  373.9 34.1 %copy-start.2 = (bf16[160,2048]{1,0:T(8,128)(2,1)S(1)}, bf16[160,2048]{1,0:T(8,128)(2,1)}, u32[]{:S(2)}) copy-start(bf16[160,2048]{1,0:T(8,128)(2,1)} %multiply_convert_fusion.2) | copy-start | bytes 1966084
  373.9 63.8 %all-gather.19.cloned.1.call-start = ((), (), s32[]{:S(2)}) async-start(), calls=%async_computation.6 | async-start | bytes 3276800 | tf_op jit(solution)/shard_map/all_gather | solution.py:26
  408.0 2.9 copy-start.9
  412.1 98.7 %reduce-scatter.14.cloned.1.call-start = ((), (), s32[]{:S(2)}) async-start(), calls=%async_computation.13 | async-start | bytes 3276800 | tf_op jit(solution)/shard_map/reduce_scatter | solution.py:90
  442.4 3.2 copy-start.11
  446.6 3.1 copy-start.8
  450.8 3.4 copy-start.5
  476.2 35.9 %copy-start.1 = (bf16[160,2048]{1,0:T(8,128)(2,1)S(1)}, bf16[160,2048]{1,0:T(8,128)(2,1)}, u32[]{:S(2)}) copy-start(bf16[160,2048]{1,0:T(8,128)(2,1)} %multiply_convert_fusion.1) | copy-start | bytes 1966084
  (10 other events, 16.5 us)
Sparse Core Ops, SparseCore 0:
  8.9 57.4 all-gather.20
  69.7 53.5 all-gather.22
  126.5 53.5 all-gather.24
  181.5 24.2 all-gather.12
  207.2 37.0 all-gather.26
  278.3 33.4 reduce-scatter.9
  315.1 25.5 all-gather.14
  342.2 27.9 all-gather.16
  374.1 33.8 reduce-scatter.11
  412.2 25.5 all-gather.18
  476.3 34.4 reduce-scatter.13
